TPU v7x, 32 devices: a whole 2x2x4 slice. The times are simulated.
32 devices in a mesh: sp: 4 (over z), fs: 4 (over y, x), tp: 2 (over core).
Axes of the slice: x: 2, y: 2, z: 4, core: 2. Of those that a mesh axis runs over, the one named last changes fastest.
Arguments:
- inputs: bfloat16 [4, 2048, 2048], P('fs', 'sp', 'tp'), may hold values from -6 to 6
- norm_gain: float32 [2048], replicated, may hold values from 0.1 to 1.9
- query_weight: bfloat16 [2048, 1024], P(('sp', 'fs'), 'tp'), may hold values from -0.125 to 0.125
- key_weight: bfloat16 [2048, 1024], P(('sp', 'fs'), 'tp'), may hold values from -0.125 to 0.125
- value_weight: bfloat16 [2048, 1024], P(('sp', 'fs'), 'tp'), may hold values from -0.125 to 0.125
- query_gain: float32 [64], replicated, may hold values from 0.8 to 7
- key_gain: float32 [64], replicated, may hold values from 0.8 to 7
- mix_lambda: float32 [8], replicated, may hold values from 0.3 to 0.8
- head_gain: float32 [128], replicated, may hold values from 0.1 to 1.9
- post_gate_weight: bfloat16 [2048, 2048], P(('sp', 'fs'), 'tp'), may hold values from -0.125 to 0.125
- pre_gate_weight: bfloat16 [2048, 2048], P(('sp', 'fs'), 'tp'), may hold values from -0.125 to 0.125
- inner_weight: bfloat16 [2048, 2048], P(('sp', 'fs'), 'tp'), may hold values from -0.125 to 0.125
- conv_taps: float32 [3, 2048], replicated, may hold values from -3 to 3
- attn_out_weight: bfloat16 [2048, 1024], P(('sp', 'fs'), 'tp'), may hold values from -0.109375 to 0.109375
- conv_out_weight: bfloat16 [2048, 2048], P(('sp', 'fs'), 'tp'), may hold values from -0.109375 to 0.109375
Outputs:
- mixed: bfloat16 [4, 2048, 2048], P('fs', ('sp', 'tp'))
All inputs are finite; a program needn't handle non-finite values.
Results may differ from a plain program's by a relative error of at most 0.015.
The roundings to bfloat16 on the way count: a program that leaves them out, or rounds other values in their place, can miss the bound.
Values may be sent and summed in bfloat16 or wider, within the bound.
A program may use at most 128 MiB of HBM per device.

v0:
```python
import math
import jax
import jax.numpy as jnp
from jax import lax
from jax.sharding import PartitionSpec as P

epsilon = 1e-06


def padded_2(x, sides, width):
    for axis, dim in sides:
        size, length = (lax.axis_size(axis), x.shape[dim])
        up = [(i, (i + 1) % size) for i in range(size - 1)]
        down = [(j, i) for i, j in up]
        last = lax.slice_in_dim(x, length - width, length, axis=dim)
        initial = lax.slice_in_dim(x, 0, width, axis=dim)
        before = lax.ppermute(last, axis, up)
        after = lax.ppermute(initial, axis, down)
        x = jnp.concatenate([before, x, after], axis=dim)
    return x


def scale_rows(values, gain):
    return values * lax.rsqrt(jnp.mean(values * values, axis=-1, keepdims=True) + epsilon) * gain


def project_all(normed, weights, products):
    result = []
    for member in range(len(weights)):
        if member < products:
            result.append(jnp.dot(normed, weights[member], preferred_element_type=jnp.float32))
        else:
            result.append(weights[member])
    return tuple(result)


def attention_branch(query, key, values, weight_two, query_gain, key_gain, head_gain):
    tok_rows = query.shape[0]
    vsize = head_gain.shape[0]
    half = query_gain.shape[0]
    heads = values.shape[1] // vsize
    query_normed = scale_rows(query.reshape(tok_rows, heads, 2, half), query_gain).astype(
        jnp.bfloat16
    )
    key_normed = scale_rows(key.reshape(tok_rows, heads * 2, half), key_gain).astype(jnp.bfloat16)
    key_normed = key_normed.reshape(tok_rows, heads * 2 * half)
    scale = half ** (-0.5)
    initial = (
        jnp.full((heads, 2, tok_rows), -1e30, jnp.float32),
        jnp.zeros((heads, 2, tok_rows), jnp.float32),
        jnp.zeros((heads, 2, tok_rows, vsize), jnp.float32),
    )
    carry = initial
    key_piece = lax.all_gather(key_normed, "sp", axis=0, tiled=True)
    value_piece = lax.all_gather(values, "sp", axis=0, tiled=True)
    length = key_piece.shape[0]
    block = math.gcd(length, 512)
    key_blocks = key_piece.reshape(length // block, block, heads, 2, half)
    value_blocks = value_piece.reshape(length // block, block, heads, vsize)

    def one_block(state, blocks):
        peak, total, accum = state
        key_block, value_block = blocks
        scores = (
            jnp.einsum(
                "qhjd,khjd->hjqk", query_normed, key_block, preferred_element_type=jnp.float32
            )
            * scale
        )
        new_peak = jnp.maximum(peak, jnp.max(scores, axis=-1))
        factor = jnp.exp(peak - new_peak)
        expo = jnp.exp(scores - new_peak[..., None])
        total = total * factor + jnp.sum(expo, axis=-1)
        accum = accum * factor[..., None] + jnp.einsum(
            "hjqk,khd->hjqd",
            expo.astype(jnp.bfloat16),
            value_block,
            preferred_element_type=jnp.float32,
        )
        return ((new_peak, total, accum), None)

    carry, unused = lax.scan(one_block, carry, (key_blocks, value_blocks))
    peak, total, accum = carry
    mapped = accum / total[..., None]
    head_out = mapped[:, 0] - weight_two[:, None, None] * mapped[:, 1]
    normed_out = scale_rows(head_out, head_gain).astype(jnp.bfloat16)
    return jnp.transpose(normed_out, (1, 0, 2)).reshape(tok_rows, heads * vsize)


def per_device(
    inputs,
    norm_gain,
    query_weight,
    key_weight,
    value_weight,
    query_gain,
    key_gain,
    mix_lambda,
    head_gain,
    post_gate_weight,
    pre_gate_weight,
    inner_weight,
    conv_taps,
    attn_out_weight,
    conv_out_weight,
):
    tokens = inputs[0]
    whole = lax.all_gather(tokens, "tp", axis=1, tiled=True)
    normed = scale_rows(whole.astype(jnp.float32), norm_gain).astype(jnp.bfloat16)
    heads_dev = value_weight.shape[1] // head_gain.shape[0]
    channels = post_gate_weight.shape[1]
    tp_index = lax.axis_index("tp")
    weight_two = lax.dynamic_slice_in_dim(mix_lambda, tp_index * heads_dev, heads_dev)
    taps = lax.dynamic_slice_in_dim(conv_taps, tp_index * channels, channels, 1)
    every_full = (
        lax.all_gather(query_weight, ("sp", "fs"), axis=0, tiled=True),
        lax.all_gather(key_weight, ("sp", "fs"), axis=0, tiled=True),
        lax.all_gather(value_weight, ("sp", "fs"), axis=0, tiled=True),
        lax.all_gather(post_gate_weight, ("sp", "fs"), axis=0, tiled=True),
        lax.all_gather(pre_gate_weight, ("sp", "fs"), axis=0, tiled=True),
        lax.all_gather(inner_weight, ("sp", "fs"), axis=0, tiled=True),
        lax.all_gather(attn_out_weight, ("sp", "fs"), axis=0, tiled=True),
        lax.all_gather(conv_out_weight, ("sp", "fs"), axis=0, tiled=True),
    )
    query, key, value_proj, post, pre_gate, inner, attn_out_full, conv_out_full = project_all(
        normed, every_full[0:3] + every_full[3:6] + every_full[6:8], 6
    )
    attn_hidden = attention_branch(
        query, key, value_proj.astype(jnp.bfloat16), weight_two, query_gain, key_gain, head_gain
    )
    post_mid = post.astype(jnp.bfloat16)
    post_wide = lax.optimization_barrier(post_mid).astype(jnp.float32)
    signal = (pre_gate * inner).astype(jnp.bfloat16)
    padded = padded_2(signal, (("sp", 0),), 1)
    shifted = lax.optimization_barrier(padded).astype(jnp.float32)
    filtered = taps[0] * shifted[:-2] + taps[1] * shifted[1:-1] + taps[2] * shifted[2:]
    conv_hidden = (post_wide * filtered).astype(jnp.bfloat16)
    contract = (((1,), (1,)), ((), ()))
    summed = lax.psum_scatter(
        (
            lax.dot_general(
                attn_hidden, attn_out_full, contract, preferred_element_type=jnp.float32
            )
            + lax.dot_general(
                conv_hidden, conv_out_full, contract, preferred_element_type=jnp.float32
            )
        ).astype(jnp.bfloat16),
        "tp",
        scatter_dimension=0,
        tiled=True,
    )
    return summed[None]


def solution(mesh):
    placed = (
        P("fs", "sp", "tp"),
        P(),
        P(("sp", "fs"), "tp"),
        P(("sp", "fs"), "tp"),
        P(("sp", "fs"), "tp"),
        P(),
        P(),
        P(),
        P(),
        P(("sp", "fs"), "tp"),
        P(("sp", "fs"), "tp"),
        P(("sp", "fs"), "tp"),
        P(),
        P(("sp", "fs"), "tp"),
        P(("sp", "fs"), "tp"),
    )
    return jax.shard_map(
        per_device,
        mesh=mesh,
        in_specs=placed,
        out_specs=P("fs", ("sp", "tp"), None),
        check_vma=False,
    )
```

profile of v0, /device:TPU:0, one launch (start us, length us, event | category | flops | bytes accessed | tf_op | source)
XLA Modules:
  0.0 693.1 jit_solution(11032667689516088220)
XLA Ops:
  10.1 12.1 %all-gather.33.cloned.1.call-done = bf16[1,512,2048]{2,1,0:T(8,128)(2,1)} async-done(((bf16[1,512,1024]{2,1,0:T(8,128)(2,1)}), bf16[1,512,2048]{2,1,0:T(8,128)(2,1)}) %all-gather.33.cloned.1.call-update) | async-done | bytes 2097168 | tf_op jit(solution)/shard_map/all_gather | solution.py:108
  24.4 62.1 %all-gather.13.cloned.1.call-done = bf16[2048,512]{1,0:T(8,128)(2,1)} async-done(((bf16[128,512]{1,0:T(8,128)(2,1)}), bf16[2048,512]{1,0:T(8,128)(2,1)}) %all-gather.13.cloned.1.call-update) | async-done | bytes 2097168 | tf_op jit(solution)/shard_map/all_gather | solution.py:117
  90.6 57.9 %all-gather.19.cloned.1.call-done = bf16[2048,512]{1,0:T(8,128)(2,1)} async-done(((bf16[128,512]{1,0:T(8,128)(2,1)}), bf16[2048,512]{1,0:T(8,128)(2,1)}) %all-gather.19.cloned.1.call-update) | async-done | bytes 2097168 | tf_op jit(solution)/shard_map/all_gather | solution.py:118
  148.6 3.7 convolution_convert_fusion.1
  157.1 53.3 %all-gather.17.cloned.1.call-done = bf16[2048,512]{1,0:T(8,128)(2,1)} async-done(((bf16[128,512]{1,0:T(8,128)(2,1)}), bf16[2048,512]{1,0:T(8,128)(2,1)}) %all-gather.17.cloned.1.call-update) | async-done | bytes 2097168 | tf_op jit(solution)/shard_map/all_gather | solution.py:116
  210.4 3.6 multiply_reduce_fusion.1
  214.3 42.0 %all-gather.15.cloned.1.call-done = bf16[2048,512]{0,1:T(8,128)(2,1)} async-done(((bf16[512,512]{0,1:T(8,128)(2,1)}), bf16[2048,512]{0,1:T(8,128)(2,1)}) %all-gather.15.cloned.1.call-update) | async-done | bytes 2097168 | tf_op jit(solution)/shard_map/all_gather | solution.py:54
  256.3 4.5 reshape.57
  260.8 3.4 copy.21
  264.2 38.0 %all-gather.21.cloned.1.call-done = bf16[2048,512]{1,0:T(8,128)(2,1)} async-done(((bf16[512,512]{1,0:T(8,128)(2,1)}), bf16[2048,512]{1,0:T(8,128)(2,1)}) %all-gather.21.cloned.1.call-update) | async-done | bytes 2097168 | tf_op jit(solution)/shard_map/all_gather | solution.py:55
  302.2 4.0 reshape.59
  306.2 59.2 %while.15 = (s32[]{:T(128)}, f32[4,2,512]{2,1,0:T(2,128)S(1)}, f32[4,2,512]{2,1,0:T(2,128)S(1)}, f32[4,2,512,128]{3,2,1,0:T(8,128)S(1)}, bf16[4,512,4,2,64]{1,4,...) while((s32[]{:T(128)}, f32[4,2,512]{2,1,0:T(2,128)S(1)}, ...), condition=%wide.region_6.7_spmd.clone, body=%wide.region_3.6_spmd.clone.sunk | while | flops 823676928 | bytes 65798792 | solution.py:82
  306.2 5.6 bitcast_reduce_fusion.3
  311.9 5.1 fusion.62
  321.0 5.6 bitcast_reduce_fusion.3
  326.7 5.0 fusion.62
  335.8 5.6 bitcast_reduce_fusion.3
  341.4 5.0 fusion.62
  350.5 5.8 bitcast_reduce_fusion.3
  356.3 5.0 fusion.62
  370.1 9.3 %all-gather.27.cloned.1.call-done = bf16[2048,1024]{1,0:T(8,128)(2,1)} async-done(((bf16[128,1024]{1,0:T(8,128)(2,1)}), bf16[2048,1024]{1,0:T(8,128)(2,1)}) %all-gather.27.cloned.1.call-update) | async-done | bytes 4194320 | tf_op jit(solution)/shard_map/all_gather | solution.py:120
  379.4 5.9 fusion.34
  385.3 71.1 %all-gather.29.cloned.1.call-done = bf16[2048,1024]{1,0:T(8,128)(2,1)} async-done(((bf16[128,1024]{1,0:T(8,128)(2,1)}), bf16[2048,1024]{1,0:T(8,128)(2,1)}) %all-gather.29.cloned.1.call-update) | async-done | bytes 4194320 | tf_op jit(solution)/shard_map/all_gather | solution.py:121
  456.4 5.2 multiply_convert_fusion
  462.6 3.4 collective-permute-start
  467.5 65.9 %all-gather.25.cloned.1.call-done = bf16[2048,1024]{1,0:T(8,128)(2,1)} async-done(((bf16[128,1024]{1,0:T(8,128)(2,1)}), bf16[2048,1024]{1,0:T(8,128)(2,1)}) %all-gather.25.cloned.1.call-update) | async-done | bytes 4194320 | tf_op jit(solution)/shard_map/all_gather | solution.py:119
  533.4 5.7 convolution_convert_fusion
  539.6 70.6 %all-gather.31.cloned.1.call-done = bf16[2048,1024]{1,0:T(8,128)(2,1)} async-done(((bf16[128,1024]{1,0:T(8,128)(2,1)}), bf16[2048,1024]{1,0:T(8,128)(2,1)}) %all-gather.31.cloned.1.call-update) | async-done | bytes 4194320 | tf_op jit(solution)/shard_map/all_gather | solution.py:123
  610.2 7.1 %fusion.24 = f32[512,2048]{1,0:T(8,128)} fusion(bf16[2048,1024]{1,0:T(8,128)(2,1)} %all-gather.31.cloned.1.call-done, f32[514,1024]{1,0:T(8,128)S(1)} %convert_element_type.49, bf16[512,1024]{1,0:T(8,128)(2,1)} %convolution_convert_fusion, f32[1024]{0:T(1024)S(1)} %bitcast.100, f32[1024]{0:T(1024)S(1)} %bitcast.99, f32[1024]{0:T(1024)S(1)} %bitcast.98), kind=kOutput, calls=%fused_computation.39 | convolution fusion | flops 2151677952 | bytes 15740928 | tf_op jit(solution)/shard_map/dot_general | solution.py:144
  617.4 54.7 %all-gather.23.cloned.1.call-done = bf16[2048,512]{1,0:T(8,128)(2,1)} async-done(((bf16[128,512]{1,0:T(8,128)(2,1)}), bf16[2048,512]{1,0:T(8,128)(2,1)}) %all-gather.23.cloned.1.call-update) | async-done | bytes 2097168 | tf_op jit(solution)/shard_map/all_gather | solution.py:122
  672.0 5.5 add_convert_fusion
  677.6 8.7 %reduce-scatter.2.cloned.1.call-done = bf16[256,2048]{1,0:T(8,128)(2,1)} async-done(((bf16[512,2048]{1,0:T(8,128)(2,1)}), bf16[256,2048]{1,0:T(8,128)(2,1)}) %reduce-scatter.2.cloned.1.call-update) | async-done | bytes 1048592 | tf_op jit(solution)/shard_map/reduce_scatter | solution.py:139
  (94 shorter events, 38.7 us)
Async XLA Ops:
  6.5 80.0 %copy-start.7 = (f32[2048]{0:T(1024)S(1)}, f32[2048]{0:T(1024)}, u32[]{:S(2)}) copy-start(f32[2048]{0:T(1024)} %param.18) | copy-start | bytes 24580
  6.5 15.7 %all-gather.33.cloned.1.call-start = ((), (), s32[]{:S(2)}) async-start(), calls=%async_computation.12 | async-start | bytes 3145728 | tf_op jit(solution)/shard_map/all_gather | solution.py:108
  7.3 79.3 %all-gather.13.cloned.1.call-start = ((), (), s32[]{:S(2)}) async-start(), calls=%async_computation.1 | async-start | bytes 2228224 | tf_op jit(solution)/shard_map/all_gather | solution.py:117
  8.0 140.5 %all-gather.19.cloned.1.call-start = ((), (), s32[]{:S(2)}) async-start(), calls=%async_computation.4 | async-start | bytes 2228224 | tf_op jit(solution)/shard_map/all_gather | solution.py:118
  8.7 201.6 %all-gather.17.cloned.1.call-start = ((), (), s32[]{:S(2)}) async-start(), calls=%async_computation.3 | async-start | bytes 2228224 | tf_op jit(solution)/shard_map/all_gather | solution.py:116
  9.3 247.0 %all-gather.15.cloned.1.call-start = ((), (), s32[]{:S(2)}) async-start(), calls=%async_computation.2 | async-start | bytes 2621440 | tf_op jit(solution)/shard_map/all_gather | solution.py:54
  22.2 64.4 %copy-start.1 = (bf16[1,512,2048]{2,1,0:T(8,128)(2,1)S(1)}, bf16[1,512,2048]{2,1,0:T(8,128)(2,1)}, u32[]{:S(2)}) copy-start(bf16[1,512,2048]{2,1,0:T(8,128)(2,1)} %all-gather.33.cloned.1.call-done) | copy-start | bytes 6291460
  90.6 65.5 %copy-start.8 = (f32[8]{0:T(128)S(1)}, f32[8]{0:T(128)}, u32[]{:S(2)}) copy-start(f32[8]{0:T(128)} %param.24) | copy-start | bytes 100
  90.6 211.6 %all-gather.21.cloned.1.call-start = ((), (), s32[]{:S(2)}) async-start(), calls=%async_computation.5 | async-start | bytes 2621440 | tf_op jit(solution)/shard_map/all_gather | solution.py:55
  152.3 227.1 %all-gather.27.cloned.1.call-start = ((), (), s32[]{:S(2)}) async-start(), calls=%async_computation.8 | async-start | bytes 4456448 | tf_op jit(solution)/shard_map/all_gather | solution.py:120
  153.0 303.4 %all-gather.29.cloned.1.call-start = ((), (), s32[]{:S(2)}) async-start(), calls=%async_computation.9 | async-start | bytes 4456448 | tf_op jit(solution)/shard_map/all_gather | solution.py:121
  153.8 379.6 %all-gather.25.cloned.1.call-start = ((), (), s32[]{:S(2)}) async-start(), calls=%async_computation.7 | async-start | bytes 4456448 | tf_op jit(solution)/shard_map/all_gather | solution.py:119
  154.5 455.7 %all-gather.31.cloned.1.call-start = ((), (), s32[]{:S(2)}) async-start(), calls=%async_computation.10 | async-start | bytes 4456448 | tf_op jit(solution)/shard_map/all_gather | solution.py:123
  155.1 516.9 %all-gather.23.cloned.1.call-start = ((), (), s32[]{:S(2)}) async-start(), calls=%async_computation.6 | async-start | bytes 2228224 | tf_op jit(solution)/shard_map/all_gather | solution.py:122
  155.8 530.4 %reduce-scatter.2.cloned.1.call-start = ((), (), s32[]{:S(2)}) async-start(), calls=%async_computation.11 | async-start | bytes 3145728 | tf_op jit(solution)/shard_map/reduce_scatter | solution.py:139
  157.1 57.0 %copy-start.5 = (f32[64]{0:T(128)S(1)}, f32[64]{0:T(128)}, u32[]{:S(2)}) copy-start(f32[64]{0:T(128)} %param.22) | copy-start | bytes 772
  311.8 6.4 copy-start
  326.7 6.3 copy-start
  341.4 6.3 copy-start
  356.3 6.3 copy-start
  369.2 0.7 copy-start.6
  369.2 10.2 %copy-start.2 = (bf16[1,512,2048]{2,1,0:T(8,128)(2,1)S(1)}, bf16[1,512,2048]{2,1,0:T(8,128)(2,1)}, u32[]{:S(2)}) copy-start(bf16[1,512,2048]{2,1,0:T(8,128)(2,1)} %all-gather.33.cloned.1.call-done) | copy-start | bytes 6291460
  461.6 1.0 copy-start.3
  462.6 76.5 %collective-permute-start = (bf16[1,1024]{1,0:T(2,128)(2,1)S(1)}, bf16[1,1024]{1,0:T(2,128)(2,1)S(1)}, u32[]{:S(2)}, u32[]{:S(2)}) collective-permute-start(bf16[1,1024]{1,0:T(2,128)(2,1)S(1)} %get-tuple-element.101), channel_id=1, source_target_pairs={{0,8},{8,16},{16,24},{1,9},{9,17},{17,25},{2,10},{10,18},{18,26},{... | collective-permute-start | bytes 6152 | tf_op jit(solution)/shard_map/ppermute | solution.py:17
  466.0 73.1 %collective-permute-start.1 = (bf16[1,1024]{1,0:T(2,128)(2,1)S(1)}, bf16[1,1024]{1,0:T(2,128)(2,1)S(1)}, u32[]{:S(2)}, u32[]{:S(2)}) collective-permute-start(bf16[1,1024]{1,0:T(2,128)(2,1)S(1)} %get-tuple-element.102), channel_id=1, source_target_pairs={{8,0},{16,8},{24,16},{9,1},{17,9},{25,17},{10,2},{18,10},{26,18},{... | collective-permute-start | bytes 6152 | tf_op jit(solution)/shard_map/ppermute | solution.py:18
  533.4 5.7 copy-start.4
Sparse Core Ops, SparseCore 0:
  8.9 13.2 all-gather.32
  25.0 61.5 all-gather.12
  89.3 59.1 all-gather.18
  151.2 59.1 all-gather.16
  211.8 44.4 all-gather.14
  257.7 44.4 all-gather.20
  305.0 74.3 all-gather.26
  382.2 74.1 all-gather.28
  459.2 74.1 all-gather.24
  536.0 74.1 all-gather.30
  613.0 58.9 all-gather.22
  677.7 8.5 reduce-scatter.1
where the time goes:
time: 694 us; the launch traced here: 693 us
  waiting for transfers between devices  552 us (80%)
  matrix products  73.6 us (11%)
  other arithmetic  26.6 us (4%)
  local copies, waits for them, and re-layouts  21.7 us (3%)
  between operations  13.8 us (2%)
    all_gather x1, waiting for transfers between devices, per_device(): lax.all_gather(inner_weight, ('sp', 'fs'), axis=0, tiled=True)  71.1 us
    all_gather x1, waiting for transfers between devices, per_device(): lax.all_gather(conv_out_weight, ('sp', 'fs'), axis=0, tiled=True)  70.6 us
    all_gather x1, waiting for transfers between devices, per_device(): lax.all_gather(post_gate_weight, ('sp', 'fs'), axis=0, tiled=True)  65.9 us
    all_gather x1, waiting for transfers between devices, per_device(): lax.all_gather(key_weight, ('sp', 'fs'), axis=0, tiled=True)  62.1 us
    all_gather x1, waiting for transfers between devices, per_device(): lax.all_gather(value_weight, ('sp', 'fs'), axis=0, tiled=True)  57.9 us
    all_gather x1, waiting for transfers between devices, per_device(): lax.all_gather(attn_out_weight, ('sp', 'fs'), axis=0, tiled=True)  54.7 us
    all_gather x1, waiting for transfers between devices, per_device(): lax.all_gather(query_weight, ('sp', 'fs'), axis=0, tiled=True)  53.3 us
    all_gather x1, waiting for transfers between devices, attention_branch(): key_piece = lax.all_gather(key_normed, 'sp', axis=0, tiled=True)  42 us
  transfers between devices with their start and end apart: 14, of which 12 were waited for; matrix products, arithmetic and copies ran while one was open for 17% of the time, Pallas kernels for 0%

commit v1 on v0

--- a/solution.py
+++ b/solution.py
@@ -52,7 +52,12 @@
     )
     carry = initial
     key_piece = lax.all_gather(key_normed, "sp", axis=0, tiled=True)
-    value_piece = lax.all_gather(values, "sp", axis=0, tiled=True)
+    ring = [values]
+    for hop in range(3):
+        ring.append(lax.ppermute(ring[-1], "sp", [(dev, (dev + 1) % 4) for dev in range(4)]))
+    value_piece = jnp.roll(
+        jnp.concatenate(ring[::-1], axis=0), (lax.axis_index("sp") + 1) * ring[0].shape[0], axis=0
+    )
     length = key_piece.shape[0]
     block = math.gcd(length, 512)
     key_blocks = key_piece.reshape(length // block, block, heads, 2, half)

time: 694 us -> 658 us (0.948)
  waiting for transfers between devices: 552 us -> 509 us
    all_gather x1 -> x0, waiting for transfers between devices: 38 us -> none  [attention_branch(): value_piece = lax.all_gather(values, 'sp', axis=0, tiled=True)]
    ppermute x0 -> x3, waiting for transfers between devices: none -> 27.2 us  [attention_branch(): lax.ppermute(ring[-1], 'sp', [(dev, (dev + 1) % 4) for dev in range(4)])]
    all_gather x1, waiting for transfers between devices: 53.3 us -> 39.4 us  [per_device(): lax.all_gather(query_weight, ('sp', 'fs'), axis=0, tiled=True)]
    all_gather x1, waiting for transfers between devices: 42 us -> 31.9 us  [attention_branch(): key_piece = lax.all_gather(key_normed, 'sp', axis=0, tiled=True)]
  transfers between devices with their start and end apart: 14 -> 16, of which waited for: 12 -> 13; matrix products, arithmetic and copies ran while one was open for 17% -> 18% of each run, Pallas kernels for 0% -> 0%
where the time goes in v1:
time: 658 us; the launch traced here: 657 us
  waiting for transfers between devices  509 us (77%)
  matrix products  73.3 us (11%)
  local copies, waits for them, and re-layouts  27.5 us (4%)
  other arithmetic  26.4 us (4%)
  between operations  13.6 us (2%)
  starting transfers between devices  6.83 us (1%)
    all_gather x1, waiting for transfers between devices, per_device(): lax.all_gather(inner_weight, ('sp', 'fs'), axis=0, tiled=True)  71.1 us
    all_gather x1, waiting for transfers between devices, per_device(): lax.all_gather(conv_out_weight, ('sp', 'fs'), axis=0, tiled=True)  70.7 us
    all_gather x1, waiting for transfers between devices, per_device(): lax.all_gather(post_gate_weight, ('sp', 'fs'), axis=0, tiled=True)  65.8 us
    all_gather x1, waiting for transfers between devices, per_device(): lax.all_gather(key_weight, ('sp', 'fs'), axis=0, tiled=True)  62.3 us
    all_gather x1, waiting for transfers between devices, per_device(): lax.all_gather(attn_out_weight, ('sp', 'fs'), axis=0, tiled=True)  54.5 us
    all_gather x1, waiting for transfers between devices, per_device(): lax.all_gather(value_weight, ('sp', 'fs'), axis=0, tiled=True)  54.5 us
    all_gather x1, waiting for transfers between devices, per_device(): lax.all_gather(query_weight, ('sp', 'fs'), axis=0, tiled=True)  39.4 us
    all_gather x1, waiting for transfers between devices, attention_branch(): key_piece = lax.all_gather(key_normed, 'sp', axis=0, tiled=True)  31.9 us
  transfers between devices with their start and end apart: 16, of which 13 were waited for; matrix products, arithmetic and copies ran while one was open for 18% of the time, Pallas kernels for 0%

profile of v1, /device:TPU:0, one launch (start us, length us, event | category | flops | bytes accessed | tf_op | source)
XLA Modules:
  0.0 657.0 jit_solution(12323183303610203938)
XLA Ops:
  10.1 12.1 %all-gather.30.cloned.1.call-done = bf16[1,512,2048]{2,1,0:T(8,128)(2,1)} async-done(((bf16[1,512,1024]{2,1,0:T(8,128)(2,1)}), bf16[1,512,2048]{2,1,0:T(8,128)(2,1)}) %all-gather.30.cloned.1.call-update) | async-done | bytes 2097168 | tf_op jit(solution)/shard_map/all_gather | solution.py:113
  24.3 62.3 %all-gather.12.cloned.1.call-done = bf16[2048,512]{1,0:T(8,128)(2,1)} async-done(((bf16[128,512]{1,0:T(8,128)(2,1)}), bf16[2048,512]{1,0:T(8,128)(2,1)}) %all-gather.12.cloned.1.call-update) | async-done | bytes 2097168 | tf_op jit(solution)/shard_map/all_gather | solution.py:122
  86.6 3.6 bitcast_reduce_fusion.1
  94.1 54.5 %all-gather.18.cloned.1.call-done = bf16[2048,512]{1,0:T(8,128)(2,1)} async-done(((bf16[128,512]{1,0:T(8,128)(2,1)}), bf16[2048,512]{1,0:T(8,128)(2,1)}) %all-gather.18.cloned.1.call-update) | async-done | bytes 2097168 | tf_op jit(solution)/shard_map/all_gather | solution.py:123
  153.0 14.8 %collective-permute-done = bf16[512,512]{1,0:T(8,128)(2,1)S(1)} collective-permute-done((bf16[512,512]{1,0:T(8,128)(2,1)S(1)}, bf16[512,512]{1,0:T(8,128)(2,1)S(1)}, u32[]{:S(2)}, u32[]{:S(2)}) %collective-permute-start) | collective-permute-done | bytes 524320 | tf_op jit(solution)/shard_map/ppermute | solution.py:57
  168.9 12.4 %collective-permute-done.1 = bf16[512,512]{1,0:T(8,128)(2,1)} collective-permute-done((bf16[512,512]{1,0:T(8,128)(2,1)S(1)}, bf16[512,512]{1,0:T(8,128)(2,1)}, u32[]{:S(2)}, u32[]{:S(2)}) %collective-permute-start.1) | collective-permute-done | bytes 524320 | tf_op jit(solution)/shard_map/ppermute | solution.py:57
  181.3 39.4 %all-gather.16.cloned.1.call-done = bf16[2048,512]{1,0:T(8,128)(2,1)} async-done(((bf16[128,512]{1,0:T(8,128)(2,1)}), bf16[2048,512]{1,0:T(8,128)(2,1)}) %all-gather.16.cloned.1.call-update) | async-done | bytes 2097168 | tf_op jit(solution)/shard_map/all_gather | solution.py:121
  220.7 3.6 multiply_reduce_fusion.1
  230.7 4.0 reshape.59
  234.7 31.9 %all-gather.14.cloned.1.call-done = bf16[2048,512]{0,1:T(8,128)(2,1)} async-done(((bf16[512,512]{0,1:T(8,128)(2,1)}), bf16[2048,512]{0,1:T(8,128)(2,1)}) %all-gather.14.cloned.1.call-update) | async-done | bytes 2097168 | tf_op jit(solution)/shard_map/all_gather | solution.py:54
  266.6 4.5 reshape.57
  274.5 59.0 %while.15 = (s32[]{:T(128)}, f32[4,2,512]{2,1,0:T(2,128)S(1)}, f32[4,2,512]{2,1,0:T(2,128)S(1)}, f32[4,2,512,128]{3,2,1,0:T(8,128)S(1)}, bf16[4,512,4,2,64]{1,4,...) while((s32[]{:T(128)}, f32[4,2,512]{2,1,0:T(2,128)S(1)}, ...), condition=%wide.region_6.7_spmd.clone, body=%wide.region_3.6_spmd.clone.sunk | while | flops 823676928 | bytes 65798792 | solution.py:87
  274.5 5.6 bitcast_reduce_fusion.3
  280.1 5.0 fusion.62
  289.3 5.6 bitcast_reduce_fusion.3
  294.9 5.0 fusion.62
  304.0 5.6 bitcast_reduce_fusion.3
  309.6 5.0 fusion.62
  318.8 5.6 bitcast_reduce_fusion.3
  324.4 5.0 fusion.62
  337.8 5.8 all-gather.24.cloned.1.call-done
  343.7 5.9 fusion.34
  349.6 71.1 %all-gather.26.cloned.1.call-done = bf16[2048,1024]{1,0:T(8,128)(2,1)} async-done(((bf16[128,1024]{1,0:T(8,128)(2,1)}), bf16[2048,1024]{1,0:T(8,128)(2,1)}) %all-gather.26.cloned.1.call-update) | async-done | bytes 4194320 | tf_op jit(solution)/shard_map/all_gather | solution.py:126
  420.7 5.2 multiply_convert_fusion
  426.9 3.4 collective-permute-start.3
  431.8 65.8 %all-gather.22.cloned.1.call-done = bf16[2048,1024]{1,0:T(8,128)(2,1)} async-done(((bf16[128,1024]{1,0:T(8,128)(2,1)}), bf16[2048,1024]{1,0:T(8,128)(2,1)}) %all-gather.22.cloned.1.call-update) | async-done | bytes 4194320 | tf_op jit(solution)/shard_map/all_gather | solution.py:124
  497.6 5.7 convolution_convert_fusion
  503.9 70.7 %all-gather.28.cloned.1.call-done = bf16[2048,1024]{1,0:T(8,128)(2,1)} async-done(((bf16[128,1024]{1,0:T(8,128)(2,1)}), bf16[2048,1024]{1,0:T(8,128)(2,1)}) %all-gather.28.cloned.1.call-update) | async-done | bytes 4194320 | tf_op jit(solution)/shard_map/all_gather | solution.py:128
  574.6 7.1 %fusion.24 = f32[512,2048]{1,0:T(8,128)} fusion(bf16[2048,1024]{1,0:T(8,128)(2,1)} %all-gather.28.cloned.1.call-done, f32[514,1024]{1,0:T(8,128)S(1)} %convert_element_type.49, bf16[512,1024]{1,0:T(8,128)(2,1)} %convolution_convert_fusion, f32[1024]{0:T(1024)S(1)} %bitcast.100, f32[1024]{0:T(1024)S(1)} %bitcast.99, f32[1024]{0:T(1024)S(1)} %bitcast.98), kind=kOutput, calls=%fused_computation.39 | convolution fusion | flops 2151677952 | bytes 15740928 | tf_op jit(solution)/shard_map/dot_general | solution.py:149
  581.8 54.5 %all-gather.20.cloned.1.call-done = bf16[2048,512]{1,0:T(8,128)(2,1)} async-done(((bf16[128,512]{1,0:T(8,128)(2,1)}), bf16[2048,512]{1,0:T(8,128)(2,1)}) %all-gather.20.cloned.1.call-update) | async-done | bytes 2097168 | tf_op jit(solution)/shard_map/all_gather | solution.py:127
  636.3 5.5 add_convert_fusion
  641.8 8.7 %reduce-scatter.2.cloned.1.call-done = bf16[256,2048]{1,0:T(8,128)(2,1)} async-done(((bf16[512,2048]{1,0:T(8,128)(2,1)}), bf16[256,2048]{1,0:T(8,128)(2,1)}) %reduce-scatter.2.cloned.1.call-update) | async-done | bytes 1048592 | tf_op jit(solution)/shard_map/reduce_scatter | solution.py:144
  (110 shorter events, 48.2 us)
Async XLA Ops:
  6.5 80.0 %copy-start.9 = (f32[2048]{0:T(1024)S(1)}, f32[2048]{0:T(1024)}, u32[]{:S(2)}) copy-start(f32[2048]{0:T(1024)} %param.18) | copy-start | bytes 24580
  6.5 15.7 %all-gather.30.cloned.1.call-start = ((), (), s32[]{:S(2)}) async-start(), calls=%async_computation.11 | async-start | bytes 3145728 | tf_op jit(solution)/shard_map/all_gather | solution.py:113
  7.3 79.3 %all-gather.12.cloned.1.call-start = ((), (), s32[]{:S(2)}) async-start(), calls=%async_computation.1 | async-start | bytes 2228224 | tf_op jit(solution)/shard_map/all_gather | solution.py:122
  8.0 140.5 %all-gather.18.cloned.1.call-start = ((), (), s32[]{:S(2)}) async-start(), calls=%async_computation.4 | async-start | bytes 2228224 | tf_op jit(solution)/shard_map/all_gather | solution.py:123
  8.7 212.0 %all-gather.16.cloned.1.call-start = ((), (), s32[]{:S(2)}) async-start(), calls=%async_computation.3 | async-start | bytes 2228224 | tf_op jit(solution)/shard_map/all_gather | solution.py:121
  9.3 257.3 %all-gather.14.cloned.1.call-start = ((), (), s32[]{:S(2)}) async-start(), calls=%async_computation.2 | async-start | bytes 2621440 | tf_op jit(solution)/shard_map/all_gather | solution.py:54
  90.2 58.4 %copy-start.1 = (bf16[1,512,2048]{2,1,0:T(8,128)(2,1)S(1)}, bf16[1,512,2048]{2,1,0:T(8,128)(2,1)}, u32[]{:S(2)}) copy-start(bf16[1,512,2048]{2,1,0:T(8,128)(2,1)} %all-gather.30.cloned.1.call-done) | copy-start | bytes 6291460
  91.2 252.5 %all-gather.24.cloned.1.call-start = ((), (), s32[]{:S(2)}) async-start(), calls=%async_computation.7 | async-start | bytes 4456448 | tf_op jit(solution)/shard_map/all_gather | solution.py:125
  91.8 328.9 %all-gather.26.cloned.1.call-start = ((), (), s32[]{:S(2)}) async-start(), calls=%async_computation.8 | async-start | bytes 4456448 | tf_op jit(solution)/shard_map/all_gather | solution.py:126
  92.5 405.1 %all-gather.22.cloned.1.call-start = ((), (), s32[]{:S(2)}) async-start(), calls=%async_computation.6 | async-start | bytes 4456448 | tf_op jit(solution)/shard_map/all_gather | solution.py:124
  93.3 481.4 %all-gather.28.cloned.1.call-start = ((), (), s32[]{:S(2)}) async-start(), calls=%async_computation.9 | async-start | bytes 4456448 | tf_op jit(solution)/shard_map/all_gather | solution.py:128
  94.0 73.9 %copy-start.10 = (f32[8]{0:T(128)S(1)}, f32[8]{0:T(128)}, u32[]{:S(2)}) copy-start(f32[8]{0:T(128)} %param.24) | copy-start | bytes 100
  94.0 542.3 %all-gather.20.cloned.1.call-start = ((), (), s32[]{:S(2)}) async-start(), calls=%async_computation.5 | async-start | bytes 2228224 | tf_op jit(solution)/shard_map/all_gather | solution.py:127
  151.4 16.3 %collective-permute-start = (bf16[512,512]{1,0:T(8,128)(2,1)S(1)}, bf16[512,512]{1,0:T(8,128)(2,1)S(1)}, u32[]{:S(2)}, u32[]{:S(2)}) collective-permute-start(bf16[512,512]{1,0:T(8,128)(2,1)S(1)} %convolution_convert_fusion.1), channel_id=1, source_target_pairs={{0,8},{8,16},{16,24},{24,0},{1,9},{9,17},{17,25},{25,1},{2,10},{10... | collective-permute-start | bytes 1572872 | tf_op jit(solution)/shard_map/ppermute | solution.py:57
  167.7 56.6 %copy-start.3 = (bf16[512,512]{1,0:T(8,128)(2,1)}, bf16[512,512]{1,0:T(8,128)(2,1)S(1)}, u32[]{:S(2)}) copy-start(bf16[512,512]{1,0:T(8,128)(2,1)S(1)} %collective-permute-done) | copy-start | bytes 1572868
  167.7 13.6 %collective-permute-start.1 = (bf16[512,512]{1,0:T(8,128)(2,1)S(1)}, bf16[512,512]{1,0:T(8,128)(2,1)}, u32[]{:S(2)}, u32[]{:S(2)}) collective-permute-start(bf16[512,512]{1,0:T(8,128)(2,1)S(1)} %collective-permute-done), channel_id=1, source_target_pairs={{0,8},{8,16},{16,24},{24,0},{1,9},{9,17},{17,25},{25,1},{2,10},{10... | collective-permute-start | bytes 1572872 | tf_op jit(solution)/shard_map/ppermute | solution.py:57
  167.8 482.8 %reduce-scatter.2.cloned.1.call-start = ((), (), s32[]{:S(2)}) async-start(), calls=%async_computation.10 | async-start | bytes 3145728 | tf_op jit(solution)/shard_map/reduce_scatter | solution.py:144
  168.9 55.5 %copy-start.7 = (f32[64]{0:T(128)S(1)}, f32[64]{0:T(128)}, u32[]{:S(2)}) copy-start(f32[64]{0:T(128)} %param.22) | copy-start | bytes 772
  181.3 43.3 %collective-permute-start.2 = (bf16[512,512]{1,0:T(8,128)(2,1)}, bf16[512,512]{1,0:T(8,128)(2,1)}, u32[]{:S(2)}, u32[]{:S(2)}) collective-permute-start(bf16[512,512]{1,0:T(8,128)(2,1)} %collective-permute-done.1), channel_id=1, source_target_pairs={{0,8},{8,16},{16,24},{24,0},{1,9},{9,17},{17,25},{25,1},{2,10},{10... | collective-permute-start | bytes 1572872 | tf_op jit(solution)/shard_map/ppermute | solution.py:57
  224.3 2.5 copy-start.4
  280.1 6.3 copy-start
  294.9 6.3 copy-start
  309.6 6.3 copy-start
  324.4 6.3 copy-start
  335.4 2.2 copy-start.8
  337.2 6.4 copy-start.2
  425.9 1.0 copy-start.5
  426.9 76.5 %collective-permute-start.3 = (bf16[1,1024]{1,0:T(2,128)(2,1)S(1)}, bf16[1,1024]{1,0:T(2,128)(2,1)S(1)}, u32[]{:S(2)}, u32[]{:S(2)}) collective-permute-start(bf16[1,1024]{1,0:T(2,128)(2,1)S(1)} %get-tuple-element.101), channel_id=1, source_target_pairs={{0,8},{8,16},{16,24},{1,9},{9,17},{17,25},{2,10},{10,18},{18,26},{... | collective-permute-start | bytes 6152 | tf_op jit(solution)/shard_map/ppermute | solution.py:17
  430.3 73.1 %collective-permute-start.4 = (bf16[1,1024]{1,0:T(2,128)(2,1)S(1)}, bf16[1,1024]{1,0:T(2,128)(2,1)S(1)}, u32[]{:S(2)}, u32[]{:S(2)}) collective-permute-start(bf16[1,1024]{1,0:T(2,128)(2,1)S(1)} %get-tuple-element.102), channel_id=1, source_target_pairs={{8,0},{16,8},{24,16},{9,1},{17,9},{25,17},{10,2},{18,10},{26,18},{... | collective-permute-start | bytes 6152 | tf_op jit(solution)/shard_map/ppermute | solution.py:18
  497.6 5.7 copy-start.6
Sparse Core Ops, SparseCore 0:
  8.9 13.2 all-gather.29
  25.0 61.5 all-gather.11
  89.3 59.1 all-gather.17
  151.2 69.4 all-gather.15
  222.1 44.4 all-gather.13
  269.2 74.3 all-gather.23
  346.4 74.1 all-gather.25
  423.4 74.1 all-gather.21
  500.4 74.1 all-gather.27
  577.3 58.9 all-gather.19
  641.9 8.5 reduce-scatter.1
